TPU v7x, 32 devices: a whole 2x2x4 slice. The times are simulated.
32 devices in a mesh: kv: 8 (over z, y), tp: 4 (over x, core).
Axes of the slice: x: 2, y: 2, z: 4, core: 2. Of those that a mesh axis runs over, the one named last changes fastest.
Arguments:
- tokens: bfloat16 [16, 4096], P(None, ('kv', 'tp')), may hold values from -8 to 8
- gate_weights: bfloat16 [2, 4096, 11264], P(None, None, ('kv', 'tp')), may hold values from -0.09375 to 0.09375
- up_weights: bfloat16 [2, 4096, 11264], P(None, None, ('kv', 'tp')), may hold values from -0.09375 to 0.09375
- down_weights: bfloat16 [2, 11264, 4096], P(None, ('kv', 'tp')), may hold values from -0.4375 to 0.4375
- norm_gain: bfloat16 [3, 4096], P(None, ('kv', 'tp')), may hold values from 0.25 to 4.5
- norm_bias: bfloat16 [3, 4096], P(None, ('kv', 'tp')), may hold values from -3 to 3
- query_weight: bfloat16 [4096, 4096], P('kv', 'tp'), may hold values from -0.09375 to 0.09375
- forget_weight: bfloat16 [4096, 4096], P('kv', 'tp'), may hold values from -0.09375 to 0.09375
- input_weight: bfloat16 [4096, 4096], P('kv', 'tp'), may hold values from -0.09375 to 0.09375
- outgate_weight: bfloat16 [4096, 4096], P('kv', 'tp'), may hold values from -0.09375 to 0.09375
- lower_bound: float32 [4096], P('tp'), may hold values from 0.05 to 0.9
- head_gain: float32 [4096], P('tp'), may hold values from 0.1 to 1.9
- out_weight: bfloat16 [4096, 4096], P('tp'), may hold values from -0.25 to 0.25
- state: float32 [16, 32, 128, 128], P('kv', 'tp'), may hold values from -3 to 3
Outputs:
- mixed: bfloat16 [16, 4096], P(None, ('kv', 'tp'))
- new_state: float32 [16, 32, 128, 128], P('kv', 'tp')
All inputs are finite; a program needn't handle non-finite values.
Results may differ from a plain program's by a relative error of at most 0.022.
Values may be sent and summed in bfloat16 or wider, within the bound.
A program may use at most 64 MiB of HBM per device.

v0:
```python
import jax
import jax.numpy as jnp
from jax import lax
from jax.sharding import PartitionSpec as P

HEAD = 128
residual_scale = 8.0**0.25
norm_eps = 1e-05
head_eps = 1e-06


def whole_norm(stream, gain_row, bias_row):
    row_mean = jnp.mean(stream, axis=-1, keepdims=True)
    centred = stream - row_mean
    spread = jnp.mean(centred * centred, axis=-1, keepdims=True)
    return centred * lax.rsqrt(spread + norm_eps) * gain_row.astype(jnp.float32) + bias_row.astype(
        jnp.float32
    )


def ffn_partial(whole_rows, gate_w, up_w, down_w):
    gate_proj = jnp.dot(whole_rows, gate_w, preferred_element_type=jnp.float32)
    up_proj = jnp.dot(whole_rows, up_w, preferred_element_type=jnp.float32)
    hidden = (jax.nn.silu(gate_proj) * up_proj).astype(jnp.bfloat16)
    return jnp.dot(hidden, down_w, preferred_element_type=jnp.float32)


def local(
    tokens,
    gate_weights,
    up_weights,
    down_weights,
    norm_gain,
    norm_bias,
    query_weight,
    forget_weight,
    input_weight,
    outgate_weight,
    lower_bound,
    head_gain,
    out_weight,
    state,
):
    own_cols = tokens.shape[1]
    col_offset = lax.axis_index(("kv", "tp")) * own_cols
    whole_tokens, whole_gain, whole_bias = (
        lax.all_gather(tokens, ("kv", "tp"), axis=1, tiled=True),
        lax.all_gather(norm_gain, ("kv", "tp"), axis=1, tiled=True),
        lax.all_gather(norm_bias, ("kv", "tp"), axis=1, tiled=True),
    )

    def finish(partial_value, residual_whole, index, want_whole):
        total = lax.psum(partial_value, ("kv", "tp"))
        stream = residual_scale * residual_whole + 0.5 * total
        normed = whole_norm(stream, whole_gain[index], whole_bias[index]).astype(jnp.bfloat16)
        if want_whole:
            return normed
        return lax.dynamic_slice_in_dim(normed, col_offset, own_cols, 1)

    partial_one = ffn_partial(whole_tokens, gate_weights[0], up_weights[0], down_weights[0])
    normed_one = finish(partial_one, whole_tokens.astype(jnp.float32), 0, True)
    seq_count = state.shape[0]
    head_count = state.shape[1]
    head_cols = query_weight.shape[1]
    weight_rows = query_weight.shape[0]
    seq_offset = lax.axis_index("kv") * seq_count
    block_rows = lax.dynamic_slice_in_dim(
        normed_one, lax.axis_index("kv") * weight_rows, weight_rows, 1
    )
    weights = (query_weight, forget_weight, input_weight, outgate_weight)
    projected = lax.psum_scatter(
        jnp.concatenate(
            [jnp.dot(block_rows, weight, preferred_element_type=jnp.float32) for weight in weights],
            axis=1,
        ).astype(jnp.bfloat16),
        "kv",
        scatter_dimension=0,
        tiled=True,
    )
    query_pre = projected[:, :head_cols].astype(jnp.float32).reshape(seq_count, head_count, HEAD)
    forget_pre = (
        projected[:, head_cols : 2 * head_cols]
        .astype(jnp.float32)
        .reshape(seq_count, head_count, HEAD)
    )
    input_pre = (
        projected[:, 2 * head_cols : 3 * head_cols]
        .astype(jnp.float32)
        .reshape(seq_count, head_count, HEAD)
    )
    outgate_pre = projected[:, 3 * head_cols :].astype(jnp.float32)
    low_bound = lower_bound.reshape(head_count, HEAD)
    forget = low_bound + (1.0 - low_bound) * jax.nn.sigmoid(forget_pre)
    key_part = (1.0 - low_bound) * jax.nn.sigmoid(-forget_pre)
    updated = forget[..., None] * state + key_part[..., None] * input_pre[:, :, None, :]
    readout = jnp.einsum(
        "shd,shde->she", jax.nn.silu(query_pre), updated, precision=lax.Precision.HIGHEST
    )
    readout = readout * lax.rsqrt(jnp.mean(readout * readout, axis=-1, keepdims=True) + head_eps)
    gated_out = (
        readout.reshape(seq_count, head_cols) * head_gain * jax.nn.silu(outgate_pre)
    ).astype(jnp.bfloat16)
    mixer_part = jnp.dot(gated_out, out_weight, preferred_element_type=jnp.float32)
    head_sum = lax.psum_scatter(
        mixer_part.astype(jnp.bfloat16), "tp", scatter_dimension=1, tiled=True
    ).astype(jnp.float32)
    piece_cols = head_sum.shape[1]
    own_normed = lax.dynamic_slice_in_dim(normed_one, seq_offset, seq_count, 0)
    own_normed = lax.dynamic_slice_in_dim(
        own_normed, lax.axis_index("tp") * piece_cols, piece_cols, 1
    )
    stream_own = (residual_scale * own_normed.astype(jnp.float32) + head_sum).astype(jnp.bfloat16)
    seq_rows = lax.all_gather(stream_own, "tp", axis=1, tiled=True)
    stream_two = lax.all_gather(seq_rows, "kv", axis=0, tiled=True)
    normed_two = whole_norm(stream_two.astype(jnp.float32), whole_gain[1], whole_bias[1]).astype(
        jnp.bfloat16
    )
    partial_two = ffn_partial(normed_two, gate_weights[1], up_weights[1], down_weights[1])
    mixed = finish(partial_two, normed_two.astype(jnp.float32), 2, False)
    return (mixed, updated)


def solution(mesh):
    return jax.shard_map(
        local,
        mesh=mesh,
        in_specs=(
            P(None, ("kv", "tp")),
            P(None, None, ("kv", "tp")),
            P(None, None, ("kv", "tp")),
            P(None, ("kv", "tp"), None),
            P(None, ("kv", "tp")),
            P(None, ("kv", "tp")),
            P("kv", "tp"),
            P("kv", "tp"),
            P("kv", "tp"),
            P("kv", "tp"),
            P("tp"),
            P("tp"),
            P("tp", None),
            P("kv", "tp", None, None),
        ),
        out_specs=(P(None, ("kv", "tp")), P("kv", "tp", None, None)),
        check_vma=False,
    )
```

profile of v0, /device:TPU:0, one launch (start us, length us, event | category | flops | bytes accessed | tf_op | source)
XLA Modules:
  0.0 475.1 jit_solution(1916518418078540519)
XLA Ops:
  7.3 44.0 %all_gather.15 = bf16[16,4096]{1,0:T(8,128)(2,1)S(1)} all-gather(bf16[16,128]{1,0:T(8,128)(2,1)} %param.14), channel_id=1, replica_groups=mesh['kv'=8,'tp'=4] {'kv','tp'}, dimensions={1}, use_global_device_ids=true | all-gather | bytes 135168 | tf_op jit(solution)/shard_map/all_gather | solution.py:47
  51.2 2.7 fusion.10
  54.0 5.5 %fusion.6 = f32[16,4096]{1,0:T(8,128)} fusion(bf16[2,352,4096]{2,1,0:T(8,128)(2,1)} %param.17, bf16[16,4096]{1,0:T(8,128)(2,1)S(1)} %all_gather.15, bf16[2,4096,352]{1,2,0:T(8,128)(2,1)} %param.16, f32[16,352]{1,0:T(8,128)S(1)} %fusion.10), kind=kOutput, calls=%fused_computation.7 | convolution fusion | flops 92308480 | bytes 6182912 | tf_op jit(solution)/shard_map/dot_general | solution.py:25
  59.6 36.7 %all_gather.16 = bf16[3,4096]{1,0:T(4,128)(2,1)S(1)} all-gather(bf16[3,128]{1,0:T(4,128)(2,1)S(1)} %copy-done.6), channel_id=1, replica_groups=mesh['kv'=8,'tp'=4] {'kv','tp'}, dimensions={1}, use_global_device_ids=true | all-gather | bytes 25344 | tf_op jit(solution)/shard_map/all_gather | solution.py:48
  96.3 38.1 %all_gather.17 = bf16[3,4096]{1,0:T(4,128)(2,1)S(1)} all-gather(bf16[3,128]{1,0:T(4,128)(2,1)S(1)} %copy-done.7), channel_id=1, replica_groups=mesh['kv'=8,'tp'=4] {'kv','tp'}, dimensions={1}, use_global_device_ids=true | all-gather | bytes 25344 | tf_op jit(solution)/shard_map/all_gather | solution.py:49
  134.5 0.6 dynamic-slice
  135.7 46.7 %all-reduce.5.cloned.1.call-done = f32[16,4096]{1,0:T(8,128)} async-done(((f32[16,4096]{1,0:T(8,128)}), f32[16,4096]{1,0:T(8,128)}) %all-reduce.5.cloned.1.call-update) | async-done | bytes 262160 | tf_op jit(solution)/shard_map/psum | solution.py:53
  182.4 1.1 fusion.36
  183.5 1.2 multiply_reduce_fusion.2
  184.7 1.1 add_convert_fusion.1
  185.8 0.2 convolution_convert_fusion.3
  186.0 0.3 convolution_convert_fusion.2
  186.3 0.3 convolution_convert_fusion.1
  186.5 1.5 convolution_convert_fusion.4
  188.0 0.7 pad_maximum_fusion
  188.8 69.5 %all-reduce.9.cloned.1.call-done = bf16[16,4096]{1,0:T(8,128)(2,1)} async-done(((bf16[16,4096]{1,0:T(8,128)(2,1)}), bf16[16,4096]{1,0:T(8,128)(2,1)}) %all-reduce.9.cloned.1.call-update) | async-done | bytes 131088
  258.3 0.8 convert_bitcast_fusion
  259.1 0.8 fusion.57
  260.0 1.8 multiply_add_fusion
  261.8 1.0 fusion.83
  263.0 4.7 convolution_convert_fusion
  267.6 1.4 copy.18
  269.2 24.0 %reduce-scatter.4.cloned.1.call-done = bf16[1024,2]{1,0:T(8,128)(2,1)} async-done(((bf16[4096,2]{1,0:T(8,128)(2,1)}), bf16[1024,2]{1,0:T(8,128)(2,1)}) %reduce-scatter.4.cloned.1.call-update) | async-done | bytes 4112
  293.1 1.1 copy.19
  294.3 5.2 %all_gather.18 = bf16[2,4096]{1,0:T(2,128)(2,1)S(1)} all-gather(bf16[2,1024]{1,0:T(2,128)(2,1)S(1)} %add_convert_fusion.2), channel_id=1, replica_groups=mesh['kv'=8,'tp'=4] {'tp'}, dimensions={1}, use_global_device_ids=true | all-gather | bytes 20480 | tf_op jit(solution)/shard_map/all_gather | solution.py:113
  299.5 30.6 %all-gather = bf16[8,2,4096]{2,1,0:T(2,128)(2,1)S(1)} all-gather(bf16[1,2,4096]{2,1,0:T(2,128)(2,1)S(1)} %bitcast.107), channel_id=1, replica_groups=mesh['kv'=8,'tp'=4] {'kv'}, dimensions={0}, use_global_device_ids=true | all-gather | bytes 147456 | tf_op jit(solution)/shard_map/all_gather | solution.py:114
  330.6 2.7 fusion.4
  333.3 5.4 %fusion = f32[16,4096]{1,0:T(8,128)} fusion(bf16[2,352,4096]{2,1,0:T(8,128)(2,1)} %param.17, bf16[2,4096,352]{1,2,0:T(8,128)(2,1)} %param.16, f32[16,352]{1,0:T(8,128)S(1)} %fusion.4, f32[16,4096]{1,0:T(8,128)S(1)} %reshape.110, f32[4096]{0:T(1024)S(1)} %bitcast.101, f32[4096]{0:T(1024)S(1)} %bitcast.97, f32[16]{0:T(128)S(1)} %add_rsqrt_fusion.2, ...), kind=kOutput, calls=%fused_computation.1 | convolution fusion | flops 92636160 | bytes 6346880 | tf_op jit(solution)/shard_map/dot_general | solution.py:25
  338.9 126.6 %all-reduce.7.cloned.1.call-done = f32[16,4096]{1,0:T(8,128)} async-done(((f32[16,4096]{1,0:T(8,128)}), f32[16,4096]{1,0:T(8,128)}) %all-reduce.7.cloned.1.call-update) | async-done | bytes 262160 | tf_op jit(solution)/shard_map/psum | solution.py:53
  465.5 1.2 fusion.35
  466.7 1.2 multiply_reduce_fusion
  467.9 0.7 fusion.69
  (48 shorter events, 1.4 us)
Async XLA Ops:
  7.2 178.6 %copy-start = (bf16[512,1024]{1,0:T(8,128)(2,1)S(1)}, bf16[512,1024]{1,0:T(8,128)(2,1)}, u32[]{:S(2)}) copy-start(bf16[512,1024]{1,0:T(8,128)(2,1)} %param.21) | copy-start | bytes 3145732
  7.2 127.3 %copy-start.8 = (u32[32]{0:T(128)S(1)}, u32[32]{0:T(128)}, u32[]{:S(2)}) copy-start(u32[32]{0:T(128)} %constant.72) | copy-start | bytes 388
  7.2 52.4 %copy-start.6 = (bf16[3,128]{1,0:T(4,128)(2,1)S(1)}, bf16[3,128]{1,0:T(4,128)(2,1)}, u32[]{:S(2)}) copy-start(bf16[3,128]{1,0:T(4,128)(2,1)} %param.18) | copy-start | bytes 2308
  7.2 89.1 %copy-start.7 = (bf16[3,128]{1,0:T(4,128)(2,1)S(1)}, bf16[3,128]{1,0:T(4,128)(2,1)}, u32[]{:S(2)}) copy-start(bf16[3,128]{1,0:T(4,128)(2,1)} %param.19) | copy-start | bytes 2308
  7.2 175.2 %all-reduce.5.cloned.1.call-start = ((), (), s32[]{:S(2)}) async-start(), calls=%async_computation.1 | async-start | bytes 524288 | tf_op jit(solution)/shard_map/psum | solution.py:53
  51.2 134.8 %copy-start.2 = (bf16[512,1024]{1,0:T(8,128)(2,1)S(1)}, bf16[512,1024]{1,0:T(8,128)(2,1)}, u32[]{:S(2)}) copy-start(bf16[512,1024]{1,0:T(8,128)(2,1)} %param.22) | copy-start | bytes 3145732
  54.0 132.3 %copy-start.3 = (bf16[512,1024]{1,0:T(8,128)(2,1)S(1)}, bf16[512,1024]{1,0:T(8,128)(2,1)}, u32[]{:S(2)}) copy-start(bf16[512,1024]{1,0:T(8,128)(2,1)} %param.23) | copy-start | bytes 3145732
  54.0 134.8 %copy-start.5 = (f32[1024]{0:T(1024)S(1)}, f32[1024]{0:T(1024)}, u32[]{:S(2)}) copy-start(f32[1024]{0:T(1024)} %param.24) | copy-start | bytes 12292
  59.5 203.5 %copy-start.4 = (f32[1024]{0:T(1024)S(1)}, f32[1024]{0:T(1024)}, u32[]{:S(2)}) copy-start(f32[1024]{0:T(1024)} %param.25) | copy-start | bytes 12292
  59.5 198.8 %all-reduce.9.cloned.1.call-start = ((), (), s32[]{:S(2)}) async-start(), calls=%async_computation.4 | async-start | bytes 262144
  188.7 104.4 %reduce-scatter.4.cloned.1.call-start = ((), (), s32[]{:S(2)}) async-start(), calls=%async_computation.3 | async-start | bytes 1310720
  261.8 5.8 %copy-start.1 = (f32[2,8,128,128]{3,2,1,0:T(8,128)}, f32[2,8,128,128]{3,2,1,0:T(8,128)S(1)}, u32[]{:S(2)}) copy-start(f32[2,8,128,128]{3,2,1,0:T(8,128)S(1)} %multiply_add_fusion) | copy-start | bytes 3145732
  269.1 196.4 %all-reduce.7.cloned.1.call-start = ((), (), s32[]{:S(2)}) async-start(), calls=%async_computation.2 | async-start | bytes 524288 | tf_op jit(solution)/shard_map/psum | solution.py:53
Sparse Core Ops, SparseCore 0:
  59.6 122.7 all-reduce.4
  188.8 69.4 all-reduce.8
  269.2 23.8 reduce-scatter.3
  338.9 126.5 all-reduce.6
where the time goes:
time: 476 us; the launch traced here: 475 us
  waiting for transfers between devices  267 us (56%)
  blocking collectives  155 us (33%)
  matrix products  24.2 us (5%)
  between operations  14.6 us (3%)
  other arithmetic  11.4 us (2%)
    psum x2, waiting for transfers between devices, finish(): total = lax.psum(partial_value, ('kv', 'tp'))  173 us
    unnamed x6, waiting for transfers between devices  93.6 us
    all_gather x1, blocking collectives, local(): lax.all_gather(tokens, ('kv', 'tp'), axis=1, tiled=True)  44 us
    all_gather x1, blocking collectives, local(): lax.all_gather(norm_bias, ('kv', 'tp'), axis=1, tiled=True)  38.1 us
    all_gather x1, blocking collectives, local(): lax.all_gather(norm_gain, ('kv', 'tp'), axis=1, tiled=True)  36.7 us
    all_gather x1, blocking collectives, local(): stream_two = lax.all_gather(seq_rows, 'kv', axis=0, tiled=True)  30.6 us
    dot_general x2, matrix products, ffn_partial(): return jnp.dot(hidden, down_w, preferred_element_type=jnp.float32)  10.9 us
  transfers between devices with their start and end apart: 4, of which 4 were waited for; matrix products, arithmetic and copies ran while one was open for 0% of the time, Pallas kernels for 0%

commit v1 on v0

--- a/solution.py
+++ b/solution.py
@@ -50,7 +50,7 @@
     )
 
     def finish(partial_value, residual_whole, index, want_whole):
-        total = lax.psum(partial_value, ("kv", "tp"))
+        total = jnp.sum(lax.all_gather(partial_value, ("kv", "tp")), axis=0)
         stream = residual_scale * residual_whole + 0.5 * total
         normed = whole_norm(stream, whole_gain[index], whole_bias[index]).astype(jnp.bfloat16)
         if want_whole:

time: 476 us -> 384 us (0.81)
  waiting for transfers between devices: 267 us -> 166 us
  other arithmetic: 11.4 us -> 18.4 us
    psum x2 -> x0, waiting for transfers between devices: 173 us -> none  [finish(): total = lax.psum(partial_value, ('kv', 'tp'))]
    all_gather x0 -> x2, waiting for transfers between devices: none -> 75.6 us  [finish(): total = jnp.sum(lax.all_gather(partial_value, ('kv', 'tp')), axis=0)]
    reduce_sum x0 -> x2, other arithmetic: none -> 7.66 us  [finish(): total = jnp.sum(lax.all_gather(partial_value, ('kv', 'tp')), axis=0)]
  transfers between devices with their start and end apart: 4 -> 4, of which waited for: 4 -> 3; matrix products, arithmetic and copies ran while one was open for 0% -> 1% of each run, Pallas kernels for 0% -> 0%
where the time goes in v1:
time: 384 us; the launch traced here: 383 us
  waiting for transfers between devices  166 us (43%)
  blocking collectives  155 us (40%)
  matrix products  24 us (6%)
  other arithmetic  18.4 us (5%)
  between operations  14.6 us (4%)
  local copies, waits for them, and re-layouts  4.75 us (1%)
    unnamed x6, waiting for transfers between devices  90.1 us
    all_gather x2, waiting for transfers between devices, finish(): total = jnp.sum(lax.all_gather(partial_value, ('kv', 'tp')), axis=0)  75.6 us
    all_gather x1, blocking collectives, local(): lax.all_gather(tokens, ('kv', 'tp'), axis=1, tiled=True)  44 us
    all_gather x1, blocking collectives, local(): lax.all_gather(norm_bias, ('kv', 'tp'), axis=1, tiled=True)  38.8 us
    all_gather x1, blocking collectives, local(): lax.all_gather(norm_gain, ('kv', 'tp'), axis=1, tiled=True)  36.9 us
    all_gather x1, blocking collectives, local(): stream_two = lax.all_gather(seq_rows, 'kv', axis=0, tiled=True)  30.5 us
    dot_general x2, matrix products, ffn_partial(): return jnp.dot(hidden, down_w, preferred_element_type=jnp.float32)  10.8 us
  transfers between devices with their start and end apart: 4, of which 3 were waited for; matrix products, arithmetic and copies ran while one was open for 1% of the time, Pallas kernels for 0%

profile of v1, /device:TPU:0, one launch (start us, length us, event | category | flops | bytes accessed | tf_op | source)
XLA Modules:
  0.0 383.0 jit_solution(1239892328921686966)
XLA Ops:
  7.3 44.0 %all_gather.27 = bf16[16,4096]{1,0:T(8,128)(2,1)S(1)} all-gather(bf16[16,128]{1,0:T(8,128)(2,1)} %param.14), channel_id=1, replica_groups=mesh['kv'=8,'tp'=4] {'kv','tp'}, dimensions={1}, use_global_device_ids=true | all-gather | bytes 135168 | tf_op jit(solution)/shard_map/all_gather | solution.py:47
  51.2 2.7 fusion.10
  53.9 5.4 %fusion.6 = f32[16,4096]{1,0:T(8,128)} fusion(bf16[2,352,4096]{2,1,0:T(8,128)(2,1)} %param.17, bf16[16,4096]{1,0:T(8,128)(2,1)S(1)} %all_gather.27, bf16[2,4096,352]{1,2,0:T(8,128)(2,1)} %param.16, f32[16,352]{1,0:T(8,128)S(1)} %fusion.10), kind=kOutput, calls=%fused_computation.7 | convolution fusion | flops 92308480 | bytes 6182912 | tf_op jit(solution)/shard_map/dot_general | solution.py:25
  60.7 36.9 %all_gather.30 = bf16[3,4096]{1,0:T(4,128)(2,1)S(1)} all-gather(bf16[3,128]{1,0:T(4,128)(2,1)S(1)} %copy-done.7), channel_id=1, replica_groups=mesh['kv'=8,'tp'=4] {'kv','tp'}, dimensions={1}, use_global_device_ids=true | all-gather | bytes 25344 | tf_op jit(solution)/shard_map/all_gather | solution.py:48
  97.5 38.8 %all_gather.31 = bf16[3,4096]{1,0:T(4,128)(2,1)S(1)} all-gather(bf16[3,128]{1,0:T(4,128)(2,1)S(1)} %copy-done.8), channel_id=1, replica_groups=mesh['kv'=8,'tp'=4] {'kv','tp'}, dimensions={1}, use_global_device_ids=true | all-gather | bytes 25344 | tf_op jit(solution)/shard_map/all_gather | solution.py:49
  136.3 0.6 slice_convert_fusion.1
  136.9 0.6 slice_convert_fusion
  137.6 3.9 %reduce_sum.81 = f32[16,4096]{1,0:T(8,128)S(1)} reduce(f32[32,16,4096]{2,1,0:T(8,128)} %bitcast.97, f32[]{:T(128)} %constant.50.clone.1), dimensions={0}, to_apply=%region_0.1 | reduce | flops 2031616 | bytes 8650756 | tf_op jit(solution)/shard_map/reduce_sum | solution.py:53
  141.9 0.9 add_convert_fusion.1
  143.5 1.5 convolution_convert_fusion.4
  145.0 0.7 pad_maximum_fusion
  145.8 0.7 broadcast_subtract_fusion
  146.5 66.0 %all-reduce.3.cloned.1.call-done = bf16[16,4096]{1,0:T(8,128)(2,1)} async-done(((bf16[16,4096]{1,0:T(8,128)(2,1)}), bf16[16,4096]{1,0:T(8,128)(2,1)}) %all-reduce.3.cloned.1.call-update) | async-done | bytes 131088
  212.5 0.8 convert_bitcast_fusion
  213.3 0.8 fusion.57
  214.1 0.7 fusion.63
  214.8 1.8 multiply_add_fusion
  216.7 1.0 fusion.83
  217.8 4.7 %convolution_convert_fusion = bf16[2,4096]{1,0:T(2,128)(2,1)S(1)} fusion(bf16[1024,4096]{1,0:T(8,128)(2,1)} %param.26, f32[1,2,8,128]{3,2,1,0:T(8,128)S(1)} %multiply_bitcast_fusion, bf16[16,4096]{1,0:T(8,128)(2,1)} %all-reduce.3.cloned.1.call-done, u32[]{:T(128)S(6)} %multiply.43, u32[]{:T(128)S(6)} %convert.26, f32[1024]{0:T(1024)S(1)} %copy-done.6), kind=kOutput, calls=%fused_computation | convolution fusion | flops 16801792 | bytes 8421384 | tf_op jit(solution)/shard_map/dot_general | solution.py:103
  222.5 1.4 copy.18
  224.0 24.0 %reduce-scatter.4.cloned.1.call-done = bf16[1024,2]{1,0:T(8,128)(2,1)} async-done(((bf16[4096,2]{1,0:T(8,128)(2,1)}), bf16[1024,2]{1,0:T(8,128)(2,1)}) %reduce-scatter.4.cloned.1.call-update) | async-done | bytes 4112
  248.0 1.1 copy.19
  249.1 0.9 add_convert_fusion.2
  249.9 5.2 %all_gather.32 = bf16[2,4096]{1,0:T(2,128)(2,1)S(1)} all-gather(bf16[2,1024]{1,0:T(2,128)(2,1)S(1)} %add_convert_fusion.2), channel_id=1, replica_groups=mesh['kv'=8,'tp'=4] {'tp'}, dimensions={1}, use_global_device_ids=true | all-gather | bytes 20480 | tf_op jit(solution)/shard_map/all_gather | solution.py:113
  255.1 30.5 %all-gather.2 = bf16[8,2,4096]{2,1,0:T(2,128)(2,1)S(1)} all-gather(bf16[1,2,4096]{2,1,0:T(2,128)(2,1)S(1)} %bitcast.111), channel_id=1, replica_groups=mesh['kv'=8,'tp'=4] {'kv'}, dimensions={0}, use_global_device_ids=true | all-gather | bytes 147456 | tf_op jit(solution)/shard_map/all_gather | solution.py:114
  286.2 2.7 fusion.4
  288.9 5.4 %fusion = f32[16,4096]{1,0:T(8,128)} fusion(bf16[2,352,4096]{2,1,0:T(8,128)(2,1)} %param.17, bf16[2,4096,352]{1,2,0:T(8,128)(2,1)} %param.16, f32[16,352]{1,0:T(8,128)S(1)} %fusion.4, f32[16,4096]{1,0:T(8,128)S(1)} %reshape.112, f32[4096]{0:T(1024)S(1)} %bitcast.105, f32[4096]{0:T(1024)S(1)} %bitcast.101, f32[16]{0:T(128)S(1)} %add_rsqrt_fusion.2, ...), kind=kOutput, calls=%fused_computation.1 | convolution fusion | flops 92636160 | bytes 6346880 | tf_op jit(solution)/shard_map/dot_general | solution.py:25
  294.3 0.8 dynamic-slice.6
  295.1 0.7 dynamic-slice.7
  295.8 75.6 %all-gather.8.cloned.1.call-done = f32[512,4096]{1,0:T(8,128)} async-done(((f32[16,4096]{1,0:T(8,128)}), f32[512,4096]{1,0:T(8,128)}) %all-gather.8.cloned.1.call-update) | async-done | bytes 8388624 | tf_op jit(solution)/shard_map/all_gather | solution.py:53
  371.5 3.8 reduce_sum.87
  375.8 0.7 fusion.69
  (52 shorter events, 3.3 us)
Async XLA Ops:
  7.2 135.6 %copy-start = (bf16[512,1024]{1,0:T(8,128)(2,1)S(1)}, bf16[512,1024]{1,0:T(8,128)(2,1)}, u32[]{:S(2)}) copy-start(bf16[512,1024]{1,0:T(8,128)(2,1)} %param.21) | copy-start | bytes 3145732
  7.2 52.2 %copy-start.9 = (u32[32]{0:T(128)S(1)}, u32[32]{0:T(128)}, u32[]{:S(2)}) copy-start(u32[32]{0:T(128)} %constant.72) | copy-start | bytes 388
  7.2 53.5 %copy-start.7 = (bf16[3,128]{1,0:T(4,128)(2,1)S(1)}, bf16[3,128]{1,0:T(4,128)(2,1)}, u32[]{:S(2)}) copy-start(bf16[3,128]{1,0:T(4,128)(2,1)} %param.18) | copy-start | bytes 2308
  7.2 90.3 %copy-start.8 = (bf16[3,128]{1,0:T(4,128)(2,1)S(1)}, bf16[3,128]{1,0:T(4,128)(2,1)}, u32[]{:S(2)}) copy-start(bf16[3,128]{1,0:T(4,128)(2,1)} %param.19) | copy-start | bytes 2308
  7.2 130.4 %all-gather.6.cloned.1.call-start = ((), (), s32[]{:S(2)}) async-start(), calls=%async_computation.1 | async-start | bytes 8650752 | tf_op jit(solution)/shard_map/all_gather | solution.py:53
  59.3 83.7 %copy-start.2 = (bf16[512,1024]{1,0:T(8,128)(2,1)S(1)}, bf16[512,1024]{1,0:T(8,128)(2,1)}, u32[]{:S(2)}) copy-start(bf16[512,1024]{1,0:T(8,128)(2,1)} %param.22) | copy-start | bytes 3145732
  59.3 153.1 %all-reduce.3.cloned.1.call-start = ((), (), s32[]{:S(2)}) async-start(), calls=%async_computation.4 | async-start | bytes 262144
  137.6 5.7 %copy-start.3 = (bf16[512,1024]{1,0:T(8,128)(2,1)S(1)}, bf16[512,1024]{1,0:T(8,128)(2,1)}, u32[]{:S(2)}) copy-start(bf16[512,1024]{1,0:T(8,128)(2,1)} %param.23) | copy-start | bytes 3145732
  142.7 0.8 copy-start.4
  142.8 75.1 %copy-start.6 = (f32[1024]{0:T(1024)S(1)}, f32[1024]{0:T(1024)}, u32[]{:S(2)}) copy-start(f32[1024]{0:T(1024)} %param.25) | copy-start | bytes 12292
  145.7 102.3 %reduce-scatter.4.cloned.1.call-start = ((), (), s32[]{:S(2)}) async-start(), calls=%async_computation.3 | async-start | bytes 1310720
  216.7 5.8 %copy-start.1 = (f32[2,8,128,128]{3,2,1,0:T(8,128)}, f32[2,8,128,128]{3,2,1,0:T(8,128)S(1)}, u32[]{:S(2)}) copy-start(f32[2,8,128,128]{3,2,1,0:T(8,128)S(1)} %multiply_add_fusion) | copy-start | bytes 3145732
  217.8 68.4 %copy-start.5 = (f32[1,4096]{1,0:T(1,128)S(1)}, f32[1,4096]{1,0:T(1,128)}, u32[]{:S(2)}) copy-start(f32[1,4096]{1,0:T(1,128)} %get-tuple-element.12) | copy-start | bytes 49156
  223.9 147.5 %all-gather.8.cloned.1.call-start = ((), (), s32[]{:S(2)}) async-start(), calls=%async_computation.2 | async-start | bytes 8650752 | tf_op jit(solution)/shard_map/all_gather | solution.py:53
Sparse Core Ops, SparseCore 0:
  59.5 73.3 all-gather.5
  145.8 66.5 all-reduce.2
  224.1 23.8 reduce-scatter.3
  294.4 76.9 all-gather.7
